TPU v7x, 512 devices: a whole 4x4x16 slice. The times are simulated.
512 devices in a mesh: sp: 64 (over z, y), tp: 8 (over x, core).
Axes of the slice: x: 4, y: 4, z: 16, core: 2. Of those that a mesh axis runs over, the one named last changes fastest.
Arguments:
- tokens: bfloat16 [6144, 4, 1024], P(('sp', 'tp')), may hold values from -6 to 6
- in_gain: float32 [1024], replicated, may hold values from 0.1 to 1.9
- w_query: bfloat16 [1024, 1024], P('sp', 'tp'), may hold values from -0.1875 to 0.1875
- w_key: bfloat16 [1024, 1024], P('sp', 'tp'), may hold values from -0.1875 to 0.1875
- w_value: bfloat16 [1024, 1024], P('sp', 'tp'), may hold values from -0.1875 to 0.1875
- w_gate: bfloat16 [1024, 1024], P('sp', 'tp'), may hold values from -0.1875 to 0.1875
- w_beta: bfloat16 [1024, 8], P('sp', 'tp'), may hold values from -0.1875 to 0.1875
- conv_query: bfloat16 [4, 1024], P(None, 'tp'), may hold values from -3 to 3
- conv_key: bfloat16 [4, 1024], P(None, 'tp'), may hold values from -3 to 3
- conv_value: bfloat16 [4, 1024], P(None, 'tp'), may hold values from -3 to 3
- decay_rate: float32 [8], P('tp'), may hold values from 0.1 to 3
- out_gain: float32 [128], replicated, may hold values from 0.1 to 1.9
- w_out: bfloat16 [1024, 1024], P('tp', 'sp'), may hold values from -0.1875 to 0.1875
Outputs:
- mixed: bfloat16 [6144, 4, 1024], P(('sp', 'tp'))
All inputs are finite; a program needn't handle non-finite values.
Results may differ from a plain program's by a relative error of at most 0.02.
Values may be sent and summed in bfloat16 or wider, within the bound.
No kernel may reach another device: no remote copies, remote signals or barrier semaphores. Data moves between devices by JAX's collectives and lax.ppermute only.
A program may use at most 64 MiB of HBM per device.

v0:
```python
import math

import jax
import jax.numpy as jnp
from jax import lax
from jax.sharding import Mesh
from jax.sharding import PartitionSpec as P

BLOCK = 32
SP = ("sp_0", "sp_1")
TP = ("tp_0", "tp_1")
SP_TP = ("sp_0", "sp_1", "tp_0", "tp_1")


epsilon = 1e-06
out_epsilon = 1e-10
highest = lax.Precision.DEFAULT


def in_order(pieces, dim):
    pieces = jnp.moveaxis(pieces, 0, dim)
    dims = pieces.shape
    return pieces.reshape(*dims[:dim], dims[dim] * dims[dim + 1], *dims[dim + 2 :])


def one_gather(arrays, axis, dims):
    flat = jnp.concatenate([a.reshape(-1) for a in arrays])
    lines, at, done = lax.all_gather(flat, axis), 0, []
    for a, dim in zip(arrays, dims):
        pieces = lines[:, at : at + a.size].reshape(-1, *a.shape)
        done.append(in_order(pieces, dim))
        at += a.size
    return tuple(done)


def gather_axes(x, axes, dim):
    filled = x
    for number in range(len(axes) - 1, -1, -1):
        filled = lax.all_gather(filled, axes[number], axis=dim, tiled=True)
    return filled


def cut_rows(length, count):
    unit = 8 if length >= 8 * count else 1
    return [length // unit * k // count * unit for k in range(1, count)]


def all_blocks(x, axes, sequence):
    pieces = x
    for k in sequence:
        pieces = lax.all_gather(pieces, axes[k])
    done = sequence[::-1]
    back = [done.index(k) for k in range(len(axes))]
    pieces = pieces.transpose(*back, *range(len(axes), pieces.ndim))
    return pieces.reshape(-1, *x.shape)


def gather_at_once(x, axes, dim):
    cut = max(range(max(1, x.ndim - 1)), key=lambda d: x.shape[d])
    count, done = len(axes), []
    for leading, piece in enumerate(jnp.split(x, cut_rows(x.shape[cut], count), axis=cut)):
        if piece.size:
            sequence = [(leading - k) % count for k in range(count)]
            done.append(all_blocks(piece, axes, sequence))
    return in_order(jnp.concatenate(done, axis=cut + 1), dim)


def worked_whole(x, axes, dim, apply):
    return apply(gather_at_once(x, axes, dim), jnp.int32(0))


def as_sent(x):
    return jax.tree.map(lambda a: a.astype(jnp.bfloat16) if a.dtype == jnp.float32 else a, x)


def passed_along(x, axis, by):
    length = lax.axis_size(axis)
    pairs = [(i, i + by) for i in range(length) if 0 <= i + by < length]
    return lax.ppermute(x, axis, pairs)


def neutral_like(x, identity):
    return jax.tree.map(
        lambda a, e: jnp.broadcast_to(jnp.asarray(e, a.dtype), a.shape), x, identity
    )


def entering(x, axes, combine, identity, reverse):
    before = start = neutral_like(x, identity)
    subtotal = x
    for axis in reversed(axes):
        length, here = lax.axis_size(axis), lax.axis_index(axis)
        pieces = jax.tree.map(lambda part: lax.all_gather(part, axis), subtotal)
        inside, subtotal = start, start
        for k in reversed(range(length)) if reverse else range(length):
            passed = k > here if reverse else k < here
            subtotal = combine(subtotal, jax.tree.map(lambda part: part[k], pieces))
            inside = jax.tree.map(lambda new, old: jnp.where(passed, new, old), subtotal, inside)
        before = combine(inside, before)
    return before


def own_rows(term, span, axes):
    subtotal = term(jnp.int32(0), span * lax.axis_size(axes)).astype(jnp.bfloat16)
    for axis in axes:
        subtotal = lax.psum_scatter(subtotal, axis, scatter_dimension=0, tiled=True)
    return subtotal.astype(jnp.float32)


def unit_inverse(lower):
    size = lower.shape[-1]
    inverse = jnp.eye(size, dtype=jnp.float32) - lower
    power = jnp.matmul(lower, lower, precision=highest)
    span = 2
    while span < size:
        inverse = inverse + jnp.matmul(inverse, power, precision=highest)
        power = jnp.matmul(power, power, precision=highest)
        span = span * 2
    return inverse


def make_terms(query, keys, values, beta, rate_col):
    size = query.shape[-2]
    steps = jnp.arange(1, size + 1).astype(jnp.float32)
    cumulative = -rate_col * steps
    lower_mask = jnp.tril(jnp.ones((size, size), bool))
    strict_mask = jnp.tril(jnp.ones((size, size), bool), -1)
    decay = jnp.where(lower_mask, jnp.exp(cumulative[..., :, None] - cumulative[..., None, :]), 0.0)
    weighted = keys * beta[..., None]
    lower = jnp.where(
        strict_mask,
        jnp.einsum("...cd,...sd->...cs", weighted, keys, precision=highest) * decay,
        0.0,
    )
    inverse = unit_inverse(lower)
    update = jnp.einsum("...cs,...sv->...cv", inverse, values * beta[..., None], precision=highest)
    erase = jnp.einsum(
        "...cs,...sd->...cd", inverse, weighted * jnp.exp(cumulative)[..., None], precision=highest
    )
    scores = jnp.einsum("...cd,...sd->...cs", query, keys, precision=highest) * decay
    query_decayed = query * jnp.exp(cumulative)[..., None]
    final = cumulative[..., -1:]
    keys_decayed = keys * jnp.exp(final - cumulative)[..., None]
    return (query_decayed, keys_decayed, update, erase, scores, jnp.exp(final))


def apply_block(state, terms):
    query_decayed, keys_decayed, update, erase, scores, kept = terms
    fresh = update - jnp.einsum("...cd,...dv->...cv", erase, state, precision=highest)
    output = jnp.einsum("...cd,...dv->...cv", query_decayed, state, precision=highest)
    output = output + jnp.einsum("...cs,...sv->...cv", scores, fresh, precision=highest)
    state = state * kept[..., None] + jnp.einsum(
        "...cd,...cv->...dv", keys_decayed, fresh, precision=highest
    )
    return (state, output)


def causal_conv(pre, conv_taps, history):
    width = conv_taps.shape[0]
    extended = jnp.concatenate([history, pre], axis=0).astype(jnp.float32)
    length = pre.shape[0]
    total = jnp.zeros(pre.shape, jnp.float32)
    for tap in range(width):
        total = total + extended[tap : tap + length] * conv_taps[tap].astype(jnp.float32)
    return total


def rms_scale(values_in, gain):
    values = values_in.astype(jnp.float32)
    scaled = values * lax.rsqrt(jnp.mean(values * values, axis=-1, keepdims=True) + epsilon)
    return (scaled * gain).astype(jnp.bfloat16)


def l2_normalize(array):
    return array * lax.rsqrt(jnp.sum(array * array, axis=-1, keepdims=True) + epsilon)


def finish(outputs, out_gain, gate_pre):
    normed = (
        outputs
        * lax.rsqrt(jnp.mean(outputs * outputs, axis=-1, keepdims=True) + out_epsilon)
        * out_gain
    )
    gate = jax.nn.silu(gate_pre.astype(jnp.float32)).reshape(outputs.shape)
    return (normed * gate).astype(jnp.bfloat16).reshape(outputs.shape[0], outputs.shape[1], -1)


def compose(earlier, later):
    first_map, first_shift = earlier
    second_map, second_shift = later
    joined_map = jnp.einsum("shde,shef->shdf", second_map, first_map, precision=highest)
    joined_shift = (
        jnp.einsum("shde,shev->shdv", second_map, first_shift, precision=highest) + second_shift
    )
    return (joined_map, joined_shift)


def shards(
    tokens,
    in_gain,
    w_query,
    w_key,
    w_value,
    w_gate,
    w_beta,
    conv_query,
    conv_key,
    conv_value,
    decay_rate,
    out_gain,
    w_out,
):
    rows = tokens.shape[0]
    seq_count = tokens.shape[1]
    width = tokens.shape[2]
    head_width = w_query.shape[1]
    local_heads = w_beta.shape[1]
    depth = head_width // local_heads
    normed = rms_scale(tokens, in_gain)
    full_query, full_key, full_value, full_gate, full_beta = one_gather(
        (w_query, w_key, w_value, w_gate, w_beta), SP, (0, 0, 0, 0, 0)
    )
    full_out = gather_axes(w_out, SP, 1)

    def project(piece, start):
        flat = piece.reshape(-1, width)
        parts = [
            jnp.dot(flat, weight, preferred_element_type=jnp.float32).astype(jnp.bfloat16)
            for weight in (full_query, full_key, full_value, full_gate, full_beta)
        ]
        return jnp.concatenate(parts, axis=1).reshape(piece.shape[0], seq_count, -1)

    projected = worked_whole(normed, TP, 0, project)
    span = projected.shape[0]
    mixed_pre = projected[:, :, : 3 * head_width]
    gate_pre = projected[:, :, 3 * head_width : 4 * head_width]
    beta_pre = projected[:, :, 4 * head_width :]
    taps = conv_query.shape[0]
    history = passed_along(as_sent(mixed_pre[span - taps + 1 :]), SP, 1)
    conv_taps = jnp.concatenate([conv_query, conv_key, conv_value], axis=1)
    convolved = jax.nn.silu(causal_conv(mixed_pre, conv_taps, history))

    def split_heads(array):
        return array.reshape(span, seq_count, local_heads, depth)

    query = l2_normalize(split_heads(convolved[:, :, :head_width])) * depth ** (-0.5)
    keys = l2_normalize(split_heads(convolved[:, :, head_width : 2 * head_width]))
    values = split_heads(convolved[:, :, 2 * head_width :])
    total_tokens = span * lax.axis_size(SP)
    beta = jax.nn.sigmoid(beta_pre.astype(jnp.float32) + math.log(depth / (4.0 * total_tokens)))
    rate_col = (decay_rate / total_tokens)[:, None]
    blocks = span // BLOCK

    def to_blocks(array):
        return jnp.moveaxis(array.reshape(blocks, BLOCK, seq_count, local_heads, depth), 1, 3)

    beta_blocks = jnp.moveaxis(beta.reshape(blocks, BLOCK, seq_count, local_heads), 1, 3)
    query_decayed, keys_decayed, update, erase, scores, kept = make_terms(
        to_blocks(query), to_blocks(keys), to_blocks(values), beta_blocks, rate_col
    )
    identity = jnp.broadcast_to(
        jnp.eye(depth, dtype=jnp.float32), (seq_count, local_heads, depth, depth)
    )
    zeros = jnp.zeros((seq_count, local_heads, depth, depth), jnp.float32)
    transfer = identity
    offset = zeros
    local_outputs = []
    readouts = []
    for index in range(blocks):
        block_terms = (
            query_decayed[index],
            keys_decayed[index],
            update[index],
            erase[index],
            scores[index],
            kept,
        )
        offset_next, output = apply_block(offset, block_terms)
        local_outputs.append(output)
        reach = query_decayed[index] - jnp.einsum(
            "shct,shtd->shcd", scores[index], erase[index], precision=highest
        )
        readouts.append(jnp.einsum("shcd,shde->shce", reach, transfer, precision=highest))
        erased = jnp.einsum("shcd,shde->shce", erase[index], transfer, precision=highest)
        transfer = transfer * kept[..., None] - jnp.einsum(
            "shcd,shce->shde", keys_decayed[index], erased, precision=highest
        )
        offset = offset_next
    prefix = entering((as_sent(transfer), as_sent(offset)), SP, compose, (identity, zeros), False)
    incoming = prefix[1]
    outputs = jnp.stack(local_outputs) + jnp.einsum(
        "nshcd,shdv->nshcv", jnp.stack(readouts), incoming, precision=highest
    )
    outputs = jnp.moveaxis(outputs, 3, 1).reshape(span, seq_count, local_heads, depth)
    gated = finish(outputs, out_gain, gate_pre)

    def head_term(start, count_rows):
        block = lax.dynamic_slice_in_dim(gated, start, count_rows, 0)
        flat = block.reshape(-1, head_width)
        return jnp.dot(flat, full_out, preferred_element_type=jnp.float32).reshape(
            count_rows, seq_count, -1
        )

    summed = own_rows(head_term, rows, TP)
    return summed.astype(jnp.bfloat16)


def solution(mesh):
    finer = Mesh(mesh.devices.reshape(16, 4, 4, 2), ("sp_0", "sp_1", "tp_0", "tp_1"))
    return jax.shard_map(
        shards,
        mesh=finer,
        in_specs=(
            P(SP_TP, None, None),
            P(),
            P(SP, TP),
            P(SP, TP),
            P(SP, TP),
            P(SP, TP),
            P(SP, TP),
            P(None, TP),
            P(None, TP),
            P(None, TP),
            P(TP),
            P(),
            P(TP, SP),
        ),
        out_specs=P(SP_TP, None, None),
        check_vma=False,
    )
```

profile of v0, /device:TPU:1, one launch (start us, length us, event | category | flops | bytes accessed | tf_op | source)
XLA Modules:
  0.0 561.1 jit_solution(10700707237145528193)
XLA Ops:
  7.3 1.3 dynamic-slice
  12.5 1.0 copy-done.1
  15.7 8.3 %all-gather.2 = bf16[12,4,1024]{2,1,0:T(4,128)(2,1)S(1)} all-gather(bf16[6,4,1024]{2,1,0:T(4,128)(2,1)S(1)} %get-tuple-element.19), channel_id=4, replica_groups=mesh['sp_0'=16,'sp_1'=4,'tp_0'=4,'tp_1'=2] {'tp_1'}, dimensions={0}, use_global_device_ids=true | all-gather | bytes 147456 | tf_op jit(solution)/shard_map/all_gather | solution.py:51
  24.0 9.2 %all-gather = bf16[24,4,1024]{2,1,0:T(4,128)(2,1)S(1)} all-gather(bf16[6,4,1024]{2,1,0:T(4,128)(2,1)S(1)} %get-tuple-element.18), channel_id=2, replica_groups=mesh['sp_0'=16,'sp_1'=4,'tp_0'=4,'tp_1'=2] {'tp_0'}, dimensions={0}, use_global_device_ids=true | all-gather | bytes 245760 | tf_op jit(solution)/shard_map/all_gather | solution.py:51
  33.3 5.0 all-gather.1
  38.4 10.2 %all-gather.3 = bf16[8,6,4,1024]{3,2,1,0:T(4,128)(2,1)S(1)} all-gather(bf16[2,6,4,1024]{3,2,1,0:T(4,128)(2,1)S(1)} %bitcast.294), channel_id=5, replica_groups=mesh['sp_0'=16,'sp_1'=4,'tp_0'=4,'tp_1'=2] {'tp_0'}, dimensions={0}, use_global_device_ids=true | all-gather | bytes 491520 | tf_op jit(solution)/shard_map/all_gather | solution.py:51
  50.3 237.1 %all-reduce.5.cloned.1.call-done = bf16[525312]{0:T(1024)(128)(2,1)} async-done(((bf16[525312]{0:T(1024)(128)(2,1)}), bf16[525312]{0:T(1024)(128)(2,1)}) %all-reduce.5.cloned.1.call-update) | async-done | bytes 1050640
  287.3 2.6 reshape.857
  292.2 1.8 collective-permute-start
  298.4 10.4 %all-gather.5 = bf16[16,128,128]{2,1,0:T(8,128)(2,1)S(1)} all-gather(bf16[4,128,128]{2,1,0:T(8,128)(2,1)S(1)} %fusion.1), channel_id=7, replica_groups=mesh['sp_0'=16,'sp_1'=4,'tp_0'=4,'tp_1'=2] {'sp_1'}, dimensions={0}, use_global_device_ids=true | all-gather | bytes 655360 | tf_op jit(solution)/shard_map/all_gather | solution.py:93
  312.3 11.3 %all-gather.7 = bf16[16,128,128]{2,1,0:T(8,128)(2,1)S(1)} all-gather(bf16[4,128,128]{2,1,0:T(8,128)(2,1)S(1)} %fusion.2), channel_id=9, replica_groups=mesh['sp_0'=16,'sp_1'=4,'tp_0'=4,'tp_1'=2] {'sp_1'}, dimensions={0}, use_global_device_ids=true | all-gather | bytes 655360 | tf_op jit(solution)/shard_map/all_gather | solution.py:93
  325.3 1.1 convolution_add_fusion.23
  327.9 9.3 %all_gather.78 = bf16[128,64]{0,1:T(8,128)(2,1)S(1)} all-gather(bf16[128,16]{0,1:T(8,128)(2,1)S(1)} %copy-done.18), channel_id=1, replica_groups=mesh['sp_0'=16,'sp_1'=4,'tp_0'=4,'tp_1'=2] {'sp_1'}, dimensions={1}, use_global_device_ids=true | all-gather | bytes 20480 | tf_op jit(solution)/shard_map/all_gather | solution.py:39
  337.2 27.0 %all_gather.79 = bf16[128,1024]{0,1:T(8,128)(2,1)S(1)} all-gather(bf16[128,64]{0,1:T(8,128)(2,1)S(1)} %all_gather.78), channel_id=1, replica_groups=mesh['sp_0'=16,'sp_1'=4,'tp_0'=4,'tp_1'=2] {'sp_0'}, dimensions={1}, use_global_device_ids=true | all-gather | bytes 278528 | tf_op jit(solution)/shard_map/all_gather | solution.py:39
  367.3 0.9 convolution_bitcast_fusion.2
  369.0 18.6 %all-gather.12.cloned.1.call-done = bf16[64,128,128]{2,1,0:T(8,128)(2,1)} async-done(((bf16[4,128,128]{2,1,0:T(8,128)(2,1)}), bf16[64,128,128]{2,1,0:T(8,128)(2,1)}) %all-gather.12.cloned.1.call-update) | async-done | bytes 2097168 | tf_op jit(solution)/shard_map/all_gather | solution.py:93
  387.6 71.7 %all-gather.14.cloned.1.call-done = bf16[64,128,128]{2,1,0:T(8,128)(2,1)} async-done(((bf16[4,128,128]{2,1,0:T(8,128)(2,1)}), bf16[64,128,128]{2,1,0:T(8,128)(2,1)}) %all-gather.14.cloned.1.call-update) | async-done | bytes 2097168 | tf_op jit(solution)/shard_map/all_gather | solution.py:93
  459.3 1.3 convolution_add_fusion.26
  460.6 1.1 convolution_add_fusion.21
  461.7 1.1 convolution_add_fusion.20
  462.9 1.1 convolution_add_fusion.19
  464.0 1.1 convolution_add_fusion.18
  465.1 1.1 convolution_add_fusion.17
  467.8 1.0 fusion.9
  468.8 1.2 fusion.11
  470.1 1.3 multiply_reduce_fusion
  471.9 1.0 copy.53
  473.0 34.6 %reduce-scatter.4.cloned.1.call-done = bf16[24,4096]{1,0:T(8,128)(2,1)} async-done(((bf16[96,4096]{1,0:T(8,128)(2,1)}), bf16[24,4096]{1,0:T(8,128)(2,1)}) %reduce-scatter.4.cloned.1.call-update) | async-done | bytes 196624
  507.6 1.7 reshape.954
  509.4 1.3 dynamic-slice.1
  511.3 41.7 %all-reduce.7.cloned.1.call-done = bf16[24,4,1024]{2,1,0:T(4,128)(2,1)} async-done(((bf16[24,4,1024]{2,1,0:T(4,128)(2,1)}), bf16[24,4,1024]{2,1,0:T(4,128)(2,1)}) %all-reduce.7.cloned.1.call-update) | async-done | bytes 196624
  553.0 1.6 constant_dynamic-slice_fusion
  (164 shorter events, 25.6 us)
Async XLA Ops:
  6.5 8.8 %copy-start.21 = (bf16[4,128]{1,0:T(4,128)(2,1)S(1)}, bf16[4,128]{1,0:T(4,128)(2,1)}, u32[]{:S(2)}) copy-start(bf16[4,128]{1,0:T(4,128)(2,1)} %param.20) | copy-start | bytes 3076
  6.5 8.8 %copy-start.9 = (bf16[12,4,1024]{2,1,0:T(4,128)(2,1)S(1)}, bf16[12,4,1024]{2,1,0:T(4,128)(2,1)}, u32[]{:S(2)}) copy-start(bf16[12,4,1024]{2,1,0:T(4,128)(2,1)} %param.13) | copy-start | bytes 294916
  6.5 9.0 %copy-start.17 = (f32[1024]{0:T(1024)S(1)}, f32[1024]{0:T(1024)}, u32[]{:S(2)}) copy-start(f32[1024]{0:T(1024)} %param.14) | copy-start | bytes 12292
  6.5 280.8 %all-reduce.5.cloned.1.call-start = ((), (), s32[]{:S(2)}) async-start(), calls=%async_computation.3 | async-start | bytes 2101248
  12.0 36.7 %copy-start.22 = (bf16[4,128]{1,0:T(4,128)(2,1)S(1)}, bf16[4,128]{1,0:T(4,128)(2,1)}, u32[]{:S(2)}) copy-start(bf16[4,128]{1,0:T(4,128)(2,1)} %param.21) | copy-start | bytes 3076
  12.0 36.7 %copy-start.23 = (bf16[4,128]{1,0:T(4,128)(2,1)S(1)}, bf16[4,128]{1,0:T(4,128)(2,1)}, u32[]{:S(2)}) copy-start(bf16[4,128]{1,0:T(4,128)(2,1)} %param.22) | copy-start | bytes 3076
  12.5 1.0 copy-start.1
  13.5 374.1 %all-gather.12.cloned.1.call-start = ((), (), s32[]{:S(2)}) async-start(), calls=%async_computation.1 | async-start | bytes 2228224 | tf_op jit(solution)/shard_map/all_gather | solution.py:93
  14.2 283.1 %copy-start.19 = (f32[32]{0:T(128)}, f32[32]{0:T(128)S(1)}, u32[]{:S(2)}) copy-start(f32[32]{0:T(128)S(1)} %fusion.124) | copy-start | bytes 388
  50.0 258.8 %copy-start.14 = (bf16[128,128]{1,0:T(8,128)(2,1)}, bf16[128,128]{1,0:T(8,128)(2,1)S(1)}, u32[]{:S(2)}) copy-start(bf16[128,128]{1,0:T(8,128)(2,1)S(1)} %fusion.110) | copy-start | bytes 98308
  50.0 247.5 %copy-start.10 = (bf16[128,128]{1,0:T(8,128)(2,1)}, bf16[128,128]{1,0:T(8,128)(2,1)S(1)}, u32[]{:S(2)}) copy-start(bf16[128,128]{1,0:T(8,128)(2,1)S(1)} %fusion.107) | copy-start | bytes 98308
  292.2 2.6 collective-permute-start
  309.0 1.9 copy-start.4
  310.2 149.0 %all-gather.14.cloned.1.call-start = ((), (), s32[]{:S(2)}) async-start(), calls=%async_computation.2 | async-start | bytes 2228224 | tf_op jit(solution)/shard_map/all_gather | solution.py:93
  311.1 0.6 copy-start.12
  312.3 15.6 %copy-start.18 = (bf16[128,16]{0,1:T(8,128)(2,1)S(1)}, bf16[128,16]{0,1:T(8,128)(2,1)}, u32[]{:S(2)}) copy-start(bf16[128,16]{0,1:T(8,128)(2,1)} %param.25) | copy-start | bytes 12292
  323.8 0.6 copy-start.6
  324.4 40.3 %copy-start.20 = (f32[32]{0:T(128)S(1)}, f32[32]{0:T(128)}, u32[]{:S(2)}) copy-start(f32[32]{0:T(128)} %copy-done.19) | copy-start | bytes 388
  326.3 0.7 copy-start.8
  327.8 38.4 %copy-start.13 = (bf16[4,32,128]{2,1,0:T(8,128)(2,1)S(1)}, bf16[4,32,128]{2,1,0:T(8,128)(2,1)}, u32[]{:S(2)}) copy-start(bf16[4,32,128]{2,1,0:T(8,128)(2,1)} %copy-done.12) | copy-start | bytes 98308
  327.8 179.8 %reduce-scatter.4.cloned.1.call-start = ((), (), s32[]{:S(2)}) async-start(), calls=%async_computation.4 | async-start | bytes 983040
  337.2 29.8 %copy-start.11 = (bf16[128,128]{1,0:T(8,128)(2,1)S(1)}, bf16[128,128]{1,0:T(8,128)(2,1)}, u32[]{:S(2)}) copy-start(bf16[128,128]{1,0:T(8,128)(2,1)} %copy-done.10) | copy-start | bytes 98308
  387.6 75.3 %copy-start = (bf16[64,128,128]{2,1,0:T(8,128)(2,1)S(1)}, bf16[64,128,128]{2,1,0:T(8,128)(2,1)}, u32[]{:S(2)}) copy-start(bf16[64,128,128]{2,1,0:T(8,128)(2,1)} %all-gather.12.cloned.1.call-done) | copy-start | bytes 6291460
  459.3 6.8 %copy-start.2 = (bf16[64,128,128]{2,1,0:T(8,128)(2,1)S(1)}, bf16[64,128,128]{2,1,0:T(8,128)(2,1)}, u32[]{:S(2)}) copy-start(bf16[64,128,128]{2,1,0:T(8,128)(2,1)} %all-gather.14.cloned.1.call-done) | copy-start | bytes 6291460
  467.6 1.2 copy-start.3
  467.6 1.2 copy-start.5
  467.6 1.2 copy-start.15
  467.8 2.2 copy-start.7
  467.8 2.2 copy-start.16
  468.8 2.7 copy-start.24
  472.9 80.0 %all-reduce.7.cloned.1.call-start = ((), (), s32[]{:S(2)}) async-start(), calls=%async_computation.5 | async-start | bytes 393216
Sparse Core Ops, SparseCore 0:
  13.6 273.7 all-reduce.4
  310.4 77.1 all-gather.11
  389.7 69.5 all-gather.13
  473.0 34.5 reduce-scatter.3
  510.3 42.5 all-reduce.6
where the time goes:
time: 562 us; the launch traced here: 561 us
  waiting for transfers between devices  404 us (72%)
  blocking collectives  90.7 us (16%)
  matrix products  26.4 us (5%)
  local copies, waits for them, and re-layouts  18.4 us (3%)
  between operations  16.6 us (3%)
    unnamed x8, waiting for transfers between devices  313 us
    all_gather x2, waiting for transfers between devices, entering(): pieces = jax.tree.map(lambda part: lax.all_gather(part, axis), subtotal)  90.3 us
    all_gather x2, blocking collectives, gather_axes(): filled = lax.all_gather(filled, axes[number], axis=dim, tiled=True)  36.2 us
    all_gather x4, blocking collectives, all_blocks(): pieces = lax.all_gather(pieces, axes[k])  32.8 us
    all_gather x2, blocking collectives, entering(): pieces = jax.tree.map(lambda part: lax.all_gather(part, axis), subtotal)  21.7 us
    dot_general x21, matrix products, compose(): jnp.einsum('shde,shev->shdv', second_map, first_shift, precision=highest)  13.4 us
    unnamed x64, local copies, waits for them, and re-layouts  11.4 us
  transfers between devices with their start and end apart: 6, of which 6 were waited for; matrix products, arithmetic and copies ran while one was open for 2% of the time, Pallas kernels for 0%

commit v1 on v0

v1 whole, which is shorter than its diff:
```python
import math

import jax
import jax.numpy as jnp
from jax import lax
from jax.experimental import pallas as pl
from jax.experimental.pallas import tpu as pltpu
from jax.sharding import Mesh
from jax.sharding import PartitionSpec as P

Z = ("zh", "zl")
SP = ("zh", "zl", "y")
TP = ("x", "c")
ALL = ("zh", "zl", "y", "x", "c")

EPS = 1e-06
OUT_EPS = 1e-10
LANES = 128
CHUNK = 128
BLOCK = 32
f32 = jnp.float32
bf16 = jnp.bfloat16


def dot(a, b):
    return jnp.dot(a.astype(bf16), b.astype(bf16), preferred_element_type=f32)


def dot_t(a, b):
    return lax.dot_general(
        a.astype(bf16), b.astype(bf16), (((1,), (1,)), ((), ())), preferred_element_type=f32
    )


def dot_l(a, b):
    return lax.dot_general(
        a.astype(bf16), b.astype(bf16), (((0,), (0,)), ((), ())), preferred_element_type=f32
    )


def sigmoid(x):
    return 1.0 / (1.0 + jnp.exp(-x))


def rms_scale(values_in, gain):
    values = values_in.astype(f32)
    scaled = values * lax.rsqrt(jnp.mean(values * values, axis=-1, keepdims=True) + EPS)
    return (scaled * gain).astype(bf16)


def project_kernel(ny, nz, rows, skip, x_ref, w_ref, pre_ref, qkv_ref, out_ref):
    piece = 6 * rows

    def part(k):
        return jnp.concatenate(
            [
                w_ref[y, pl.ds(skip + z * piece + k * rows, rows), :]
                for z in range(nz)
                for y in range(ny)
            ],
            axis=0,
        )

    weights = jnp.concatenate([part(0), part(1), part(2)], axis=1)
    qkv_ref[...] = weights
    x = x_ref[...]
    pre_ref[:, : 3 * LANES] = jnp.dot(x, weights, preferred_element_type=f32).astype(bf16)
    tail = jnp.concatenate([part(3), part(5)], axis=1)
    pre_ref[:, 3 * LANES :] = jnp.dot(x, tail, preferred_element_type=f32).astype(bf16)
    out_ref[...] = part(4)


def delta_kernel(shift, pre_ref, hist_ref, w_ref, taps_ref, par_ref, o_ref, r_ref, eb_ref, ext):
    span = pre_ref.shape[0]
    width = 3 * LANES
    lam = par_ref[0:1, :]
    ext[0:8, :] = (
        jnp.dot(hist_ref[...], w_ref[...], preferred_element_type=f32).astype(bf16).astype(f32)
    )
    ext[8:, :] = pre_ref[:, :width].astype(f32)
    total = ext[5 : 5 + span, :] * taps_ref[0:1, :]
    for tap in range(1, 4):
        total = total + ext[5 + tap : 5 + tap + span, :] * taps_ref[tap : tap + 1, :]
    act = total * sigmoid(total)
    query, keys, values = act[:, :LANES], act[:, LANES : 2 * LANES], act[:, 2 * LANES :]
    query = query * (
        lax.rsqrt(jnp.sum(query * query, axis=-1, keepdims=True) + EPS) * LANES ** (-0.5)
    )
    keys = keys * lax.rsqrt(jnp.sum(keys * keys, axis=-1, keepdims=True) + EPS)
    beta = sigmoid(pre_ref[:, 4 * LANES :].astype(f32) + shift)

    shape = (CHUNK, CHUNK)
    i = lax.broadcasted_iota(jnp.int32, shape, 0)
    j = lax.broadcasted_iota(jnp.int32, shape, 1)
    row = i.astype(f32)
    decay = jnp.where(i >= j, jnp.exp(-lam * (row - j.astype(f32))), 0.0)
    strict = jnp.where(i > j, decay, 0.0)
    gamma = jnp.exp(-lam * (row + 1.0))
    toward = jnp.exp(-lam * (CHUNK - 1.0 - row))
    kept = jnp.exp(-lam * float(CHUNK))
    eye = jnp.where(i == j, 1.0, 0.0)
    same = [(i // s) == (j // s) for s in (BLOCK, 2 * BLOCK)]
    count = span // CHUNK
    ks = [keys[n * CHUNK : (n + 1) * CHUNK] for n in range(count)]
    qs = [query[n * CHUNK : (n + 1) * CHUNK] for n in range(count)]
    vs = [values[n * CHUNK : (n + 1) * CHUNK] for n in range(count)]
    bs = [beta[n * CHUNK : (n + 1) * CHUNK] for n in range(count)]
    kb = [k * b for k, b in zip(ks, bs)]
    lower = [dot_t(a, k) * strict for a, k in zip(kb, ks)]
    diag = [jnp.where(same[0], a, 0.0) for a in lower]
    inv = [eye - a for a in diag]
    power = [dot(a, a) for a in diag]
    reach = 2
    while reach < BLOCK:
        inv = [a + dot(a, p) for a, p in zip(inv, power)]
        reach *= 2
        if reach < BLOCK:
            power = [dot(p, p) for p in power]
    side = [jnp.where(same[1], jnp.where(same[0], 0.0, a), 0.0) for a in lower]
    inv = [a - dot(a, dot(s, a)) for a, s in zip(inv, side)]
    side = [jnp.where(same[1], 0.0, a) for a in lower]
    inv = [a - dot(a, dot(s, a)) for a, s in zip(inv, side)]
    uw = [
        dot(a, jnp.concatenate([v * b, k * gamma], axis=1))
        for a, v, b, k in zip(inv, vs, bs, kb)
    ]
    scores = [dot_t(q, k) * decay for q, k in zip(qs, ks)]
    su = [dot(s, a) for s, a in zip(scores, uw)]
    ku = [dot_l(k * toward, a) for k, a in zip(ks, uw)]
    local = [a[:, :LANES] for a in su]
    read = [q * gamma - a[:, LANES:] for q, a in zip(qs, su)]
    new = [a[:, :LANES] for a in ku]
    drop = [-a[:, LANES:] for a in ku]
    fmap, off = drop[0], new[0]
    o_ref[:CHUNK, :] = local[0]
    r_ref[:CHUNK, :] = read[0].astype(bf16)
    kap = kept
    for n in range(1, count):
        both = jnp.concatenate([fmap, off], axis=1)
        seen = dot(read[n], both)
        at = slice(n * CHUNK, (n + 1) * CHUNK)
        o_ref[at, :] = local[n] + seen[:, LANES:]
        r_ref[at, :] = (read[n] * kap + seen[:, :LANES]).astype(bf16)
        moved = dot(drop[n], both)
        fmap = fmap * kept + drop[n] * kap + moved[:, :LANES]
        off = off * kept + moved[:, LANES:] + new[n]
        kap = kap * kept
    eb_ref[:LANES, :] = fmap.astype(bf16)
    eb_ref[LANES:, :] = off.astype(bf16)


def group_kernel(span, g_ref, par_ref, eb_ref, prefix_ref):
    lam = par_ref[0:1, :]
    place = par_ref[1:2, :]
    count = g_ref.shape[0]
    fmap = jnp.zeros((LANES, LANES), f32)
    off = jnp.zeros((LANES, LANES), f32)
    keep_map, keep_off = fmap, off
    step = jnp.exp(-lam * float(span))
    for m in range(count):
        kap = jnp.exp(-lam * float(span * m))
        e = g_ref[m, :LANES, :]
        if m:
            moved = dot(e, jnp.concatenate([fmap, off], axis=1))
            fmap = fmap * step + e.astype(f32) * kap + moved[:, :LANES]
            off = off * step + moved[:, LANES:] + g_ref[m, LANES:, :].astype(f32)
        else:
            fmap = e.astype(f32)
            off = g_ref[m, LANES:, :].astype(f32)
        if m + 1 < count:
            here = place == float(m + 1)
            keep_map = jnp.where(here, fmap, keep_map)
            keep_off = jnp.where(here, off, keep_off)
    eb_ref[:LANES, :] = fmap.astype(bf16)
    eb_ref[LANES:, :] = off.astype(bf16)
    prefix_ref[:LANES, :] = keep_map
    prefix_ref[LANES:, :] = keep_off


def finish_kernel(span, g_ref, prefix_ref, par_ref, o_ref, r_ref, pre_ref, gain_ref, out_ref):
    lam = par_ref[0:1, :]
    low = par_ref[1:2, :]
    high = par_ref[2:3, :]
    count = g_ref.shape[0]
    step = jnp.exp(-lam * float(span * count))
    state = jnp.where(high > 0.0, g_ref[0, LANES:, :].astype(f32), 0.0)
    for m in range(1, count - 1):
        later = state * step + dot(g_ref[m, :LANES, :], state) + g_ref[m, LANES:, :].astype(f32)
        state = jnp.where(high > float(m), later, state)
    entry = (
        state * jnp.exp(-lam * (low * float(span)))
        + dot(prefix_ref[:LANES, :], state)
        + prefix_ref[LANES:, :]
    )
    out = o_ref[...] + dot(r_ref[...], entry)
    normed = out * lax.rsqrt(jnp.mean(out * out, axis=-1, keepdims=True) + OUT_EPS) * gain_ref[0:1, :]
    gate = pre_ref[:, 3 * LANES : 4 * LANES].astype(f32)
    out_ref[...] = (normed * (gate * sigmoid(gate))).astype(bf16)


def call(kernel, outs, args, flops, scratch=()):
    spec = pl.BlockSpec(memory_space=pltpu.VMEM)
    return pl.pallas_call(
        kernel,
        out_shape=outs,
        in_specs=[spec] * len(args),
        out_specs=tuple([spec] * len(outs)),
        scratch_shapes=scratch,
        cost_estimate=pl.CostEstimate(flops=flops, bytes_accessed=4 << 20, transcendentals=0),
        compiler_params=pltpu.CompilerParams(vmem_limit_bytes=40 << 20),
    )(*args)


def shards(
    tokens,
    in_gain,
    w_query,
    w_key,
    w_value,
    w_gate,
    w_beta,
    conv_query,
    conv_key,
    conv_value,
    decay_rate,
    out_gain,
    w_out,
):
    own, seqs, width = tokens.shape
    rows = w_query.shape[0]
    nz = lax.axis_size("zh") * lax.axis_size("zl")
    ny, nx, nc = lax.axis_size("y"), lax.axis_size("x"), lax.axis_size("c")
    span = own * ny * nx * nc
    total = span * nz
    piece = 6 * rows
    slot = own * width // LANES

    normed = rms_scale(tokens, in_gain)
    pack = jnp.concatenate(
        [
            w_query,
            w_key,
            w_value,
            w_gate,
            w_out.T,
            jnp.broadcast_to(w_beta, (rows, LANES)),
        ],
        axis=0,
    )
    deep = lax.all_gather(pack, Z).reshape(nz * piece, LANES)
    send = jnp.concatenate(
        [
            normed.transpose(1, 0, 2).reshape(seqs, slot, LANES),
            jnp.broadcast_to(deep, (seqs, nz * piece, LANES)),
        ],
        axis=1,
    )
    got = lax.all_to_all(send, "y", 0, 0, tiled=True)
    x = lax.all_gather(got[:, :slot], TP)
    x = x.reshape(nx * nc, ny, own, width).transpose(1, 0, 2, 3).reshape(span, width)
    pairs = [(k, k + 1) for k in range(nz - 1)]
    hist = lax.ppermute(x[span - 8 :], Z, pairs)

    pre, w_qkv, out_rows = call(
        lambda *refs: project_kernel(ny, nz, rows, slot, *refs),
        (
            jax.ShapeDtypeStruct((span, 5 * LANES), bf16),
            jax.ShapeDtypeStruct((width, 3 * LANES), bf16),
            jax.ShapeDtypeStruct((width, LANES), bf16),
        ),
        (x, got),
        2 * span * width * 5 * LANES,
    )
    out_pair = lax.all_gather(out_rows, "c")

    lam = decay_rate.astype(f32) / total
    places = jnp.stack(
        [
            lam[0],
            lax.axis_index("zl").astype(f32),
            lax.axis_index("zh").astype(f32),
        ]
    )
    par = jnp.broadcast_to(jnp.pad(places, (0, 5))[:, None], (8, LANES))
    taps = jnp.concatenate([conv_query, conv_key, conv_value], axis=1).astype(f32)
    taps = jnp.pad(taps, ((0, 4), (0, 0)))
    shift = math.log(LANES / (4.0 * total))
    local, read, eb = call(
        lambda *refs: delta_kernel(shift, *refs),
        (
            jax.ShapeDtypeStruct((span, LANES), f32),
            jax.ShapeDtypeStruct((span, LANES), bf16),
            jax.ShapeDtypeStruct((2 * LANES, LANES), bf16),
        ),
        (pre, hist, w_qkv, taps, par),
        200 << 20,
        (pltpu.VMEM((span + 8, 3 * LANES), f32),),
    )
    group = lax.all_gather(eb, "zl")
    eb_group, prefix = call(
        lambda *refs: group_kernel(span, *refs),
        (
            jax.ShapeDtypeStruct((2 * LANES, LANES), bf16),
            jax.ShapeDtypeStruct((2 * LANES, LANES), f32),
        ),
        (group, par),
        30 << 20,
    )
    groups = lax.all_gather(eb_group, "zh")
    gain = jnp.broadcast_to(out_gain[None, :], (8, LANES))
    (gated,) = call(
        lambda *refs: finish_kernel(span, *refs),
        (jax.ShapeDtypeStruct((span, LANES), bf16),),
        (groups, prefix, par, local, read, pre, gain),
        40 << 20,
    )
    halves = gated.reshape(ny * nx, nc, own, LANES).transpose(1, 0, 2, 3)
    heads = lax.all_to_all(halves, "c", 0, 0, tiled=True).reshape(nc, -1, LANES)
    part = jnp.einsum("ctd,cod->to", heads, out_pair, preferred_element_type=f32).astype(bf16)
    parts = lax.all_to_all(part.reshape(ny * nx, own, width), ("y", "x"), 0, 0, tiled=True)
    mixed = jnp.sum(parts.reshape(ny, nx, own, width).astype(f32), axis=1)
    return mixed.astype(bf16).transpose(1, 0, 2)


def solution(mesh):
    sp, tp = mesh.devices.shape
    finer = Mesh(mesh.devices.reshape(4, sp // 16, 4, tp // 2, 2), ALL)
    return jax.shard_map(
        shards,
        mesh=finer,
        in_specs=(
            P(ALL, None, None),
            P(),
            P(SP, TP),
            P(SP, TP),
            P(SP, TP),
            P(SP, TP),
            P(SP, TP),
            P(None, TP),
            P(None, TP),
            P(None, TP),
            P(TP),
            P(),
            P(TP, SP),
        ),
        out_specs=P(ALL, None, None),
        check_vma=False,
    )
```

time: 562 us -> 150 us (0.27)
  waiting for transfers between devices: 404 us -> 12.4 us
  matrix products: 26.4 us -> 0.32 us
  blocking collectives: 90.7 us -> 113 us
  between operations: 16.6 us -> 0.81 us
  local copies, waits for them, and re-layouts: 18.4 us -> 8.51 us
    unnamed x8 -> x0, waiting for transfers between devices: 313 us -> none
    all_gather x2 -> x0, waiting for transfers between devices: 90.3 us -> none  [entering(): pieces = jax.tree.map(lambda part: lax.all_gather(part, axis), subtotal)]
    dot_general x61 -> x1, matrix products: 26.4 us -> 0.32 us  [shards(): jnp.einsum('ctd,cod->to', heads, out_pair, preferred_element_type=f32)]
    all_to_all x0 -> x2, blocking collectives: none -> 25.4 us  [the longest x1 15.9 us: shards(): lax.all_to_all(part.reshape(ny * nx, own, width), ('y', 'x'), 0, 0, tiled...]
    all_to_all x0 -> x1, waiting for transfers between devices: none -> 12.4 us  [shards(): got = lax.all_to_all(send, 'y', 0, 0, tiled=True)]
    unnamed x64 -> x13, local copies, waits for them, and re-layouts: 11.4 us -> 3.48 us
    all_gather x8 -> x5, blocking collectives: 90.7 us -> 87.6 us  [the longest x1 31.1 us: shards(): deep = lax.all_gather(pack, Z).reshape(nz * piece, LANES)]
  transfers between devices with their start and end apart: 6 -> 2, of which waited for: 6 -> 1; matrix products, arithmetic and copies ran while one was open for 2% -> 0% of each run, Pallas kernels for 0% -> 1%
where the time goes in v1:
time: 150 us
  blocking collectives  113 us (75%)
  waiting for transfers between devices  12.4 us (8%)
  local copies, waits for them, and re-layouts  8.51 us (6%)
  starting transfers between devices  6.49 us (4%)
  Pallas kernels  4.71 us (3%)
  other arithmetic  3.51 us (2%)
    all_gather x1, blocking collectives, shards(): deep = lax.all_gather(pack, Z).reshape(nz * piece, LANES)  31.1 us
    all_gather x1, blocking collectives, shards(): x = lax.all_gather(got[:, :slot], TP)  23.2 us
    all_gather x1, blocking collectives, shards(): groups = lax.all_gather(eb_group, 'zh')  20.2 us
    all_to_all x1, blocking collectives, shards(): lax.all_to_all(part.reshape(ny * nx, own, width), ('y', 'x'), 0, 0, tiled...  15.9 us
    all_to_all x1, waiting for transfers between devices, shards(): got = lax.all_to_all(send, 'y', 0, 0, tiled=True)  12.4 us
    all_gather x1, blocking collectives, shards(): group = lax.all_gather(eb, 'zl')  10.9 us
    all_to_all x1, blocking collectives, shards(): heads = lax.all_to_all(halves, 'c', 0, 0, tiled=True).reshape(nc, -1, LANES)  9.49 us
    pallas_call x4, Pallas kernels, call(): pl.pallas_call(kernel, out_shape=outs, in_specs=[spec] * len(args), out_s...  4.71 us
  transfers between devices with their start and end apart: 2, of which 1 were waited for; matrix products, arithmetic and copies ran while one was open for 0% of the time, Pallas kernels for 1%

profile of v1, /device:TPU:1, one launch (start us, length us, event | category | flops | bytes accessed | tf_op | source)
XLA Modules:
  0.0 149.8 jit_solution(16345217670965857528)
XLA Ops:
  0.0 0.7 constant_dynamic-update-slice_fusion.5
  0.7 0.7 constant_dynamic-update-slice_fusion.4
  1.4 0.7 constant_dynamic-update-slice_fusion.3
  2.1 0.7 constant_dynamic-update-slice_fusion.2
  2.8 0.7 constant_dynamic-update-slice_fusion.1
  3.5 0.7 constant_dynamic-update-slice_fusion
  4.2 31.1 %all-gather = bf16[1536,128]{1,0:T(8,128)(2,1)S(1)} all-gather(bf16[96,128]{1,0:T(8,128)(2,1)S(1)} %constant_dynamic-update-slice_fusion), channel_id=2, replica_groups=mesh['zh'=4,'zl'=4,'y'=4,'x'=4,'c'=2] {'zh','zl'}, dimensions={0}, use_global_device_ids=true | all-gather | bytes 417792 | tf_op jit(solution)/shard_map/all_gather | solution.py:250
  35.3 1.0 fusion.1
  36.3 1.0 fusion.4
  37.5 0.2 broadcast_in_dim.12
  37.7 1.3 pad_maximum_fusion
  39.0 4.3 %all-to-all-start = ((bf16[4,1632,128]{2,1,0:T(8,128)(2,1)}), bf16[4,1632,128]{2,1,0:T(8,128)(2,1)S(1)}, u32[]{:S(2)}, u32[]{:S(2)}) async-start(bf16[4,1632,128]{2,1,0:T(8,128)(2,1)} %pad_maximum_fusion), calls=%async_computation | async-start | bytes 3342336 | tf_op jit(solution)/shard_map/all_to_all | solution.py:258
  44.0 12.4 %all-to-all-done.refs_1_ = bf16[4,1632,128]{2,1,0:T(8,128)(2,1)S(1)} async-done(((bf16[4,1632,128]{2,1,0:T(8,128)(2,1)}), bf16[4,1632,128]{2,1,0:T(8,128)(2,1)S(1)}, u32[]{:S(2)}, u32[]{:S(2)}) %all-to-all-start) | async-done | bytes 1671200 | tf_op jit(solution)/shard_map/all_to_all | solution.py:258
  56.5 23.2 %all-gather.1 = bf16[32,96,128]{2,1,0:T(8,128)(2,1)S(1)} all-gather(bf16[4,96,128]{2,1,0:T(8,128)(2,1)S(1)} %slice.8), channel_id=3, replica_groups=mesh['zh'=4,'zl'=4,'y'=4,'x'=4,'c'=2] {'x','c'}, dimensions={0}, use_global_device_ids=true | all-gather | bytes 884736 | tf_op jit(solution)/shard_map/all_gather | solution.py:259
  79.7 0.5 reshape.37
  80.2 1.1 copy.22
  81.3 1.3 reshape.38.refs_0_
  82.6 2.2 %collective-permute-start = (bf16[8,1024]{1,0:T(8,128)(2,1)S(1)}, bf16[8,1024]{1,0:T(8,128)(2,1)S(1)}, u32[]{:S(2)}, u32[]{:S(2)}) collective-permute-start(bf16[8,1024]{1,0:T(8,128)(2,1)S(1)} %slice.9), channel_id=1, source_target_pairs={{0,32},{32,64},{64,96},{96,128},{128,160},{160,192},{192,224},{224... | collective-permute-start | bytes 49160 | tf_op jit(solution)/shard_map/ppermute | solution.py:262
  84.8 0.8 shard_map.127
  85.6 2.3 %all-gather.4 = bf16[2048,128]{1,0:T(8,128)(2,1)S(1)} all-gather(bf16[1024,128]{1,0:T(8,128)(2,1)S(1)} %get-tuple-element.20), channel_id=6, replica_groups=mesh['zh'=4,'zl'=4,'y'=4,'x'=4,'c'=2] {'c'}, dimensions={0}, use_global_device_ids=true | all-gather | bytes 786432 | tf_op jit(solution)/shard_map/all_gather | solution.py:274
  88.0 2.8 %shard_map.128 = (f32[384,128]{1,0:T(8,128)S(1)}, bf16[384,128]{1,0:T(8,128)(2,1)S(1)}, bf16[256,128]{1,0:T(8,128)(2,1)S(1)}) custom-call(bf16[384,640]{1,0:T(8,128)(2,1)S(1)} %get-tuple-element.13.refs_0_.refs_5_, bf16[8,1024]{1,0:T(8,128)(2,1)S(1)} %collective-permute-done.refs_1_, bf16[1024,384]{1,0:T(8,128)(2,1)S(1)} %get-tuple-element.14.refs_2_, ...), custom_call_target="tpu_custom_call" | custom-call | flops 209715200 | bytes 4194304 | tf_op jit(solution)/shard_map/pallas_call | solution.py:203
  90.7 10.9 %all-gather.2 = bf16[1024,128]{1,0:T(8,128)(2,1)S(1)} all-gather(bf16[256,128]{1,0:T(8,128)(2,1)S(1)} %get-tuple-element.15), channel_id=4, replica_groups=mesh['zh'=4,'zl'=4,'y'=4,'x'=4,'c'=2] {'zl'}, dimensions={0}, use_global_device_ids=true | all-gather | bytes 327680 | tf_op jit(solution)/shard_map/all_gather | solution.py:299
  101.6 0.5 shard_map.129
  102.1 20.2 %all-gather.3 = bf16[1024,128]{1,0:T(8,128)(2,1)S(1)} all-gather(bf16[256,128]{1,0:T(8,128)(2,1)S(1)} %get-tuple-element.16), channel_id=5, replica_groups=mesh['zh'=4,'zl'=4,'y'=4,'x'=4,'c'=2] {'zh'}, dimensions={0}, use_global_device_ids=true | all-gather | bytes 327680 | tf_op jit(solution)/shard_map/all_gather | solution.py:309
  122.3 0.7 shard_map.130
  123.0 9.5 %all_to_all.15 = bf16[2,16,12,128]{3,1,2,0:T(8,128)(2,1)S(1)} all-to-all(bf16[2,16,12,128]{3,1,2,0:T(8,128)(2,1)S(1)} %copy.23), channel_id=1, replica_groups=mesh['zh'=4,'zl'=4,'y'=4,'x'=4,'c'=2] {'c'}, dimensions={0} | all-to-all | bytes 196608 | tf_op jit(solution)/shard_map/all_to_all | solution.py:318
  132.5 0.1 copy.24
  132.6 0.3 fusion
  133.0 0.1 reshape.41
  133.1 15.9 %all_to_all.16 = bf16[16,12,1024]{2,1,0:T(8,128)(2,1)S(1)} all-to-all(bf16[16,12,1024]{2,1,0:T(8,128)(2,1)S(1)} %reshape.41), channel_id=1, replica_groups=mesh['zh'=4,'zl'=4,'y'=4,'x'=4,'c'=2] {'y','x'}, dimensions={0} | all-to-all | bytes 786432 | tf_op jit(solution)/shard_map/all_to_all | solution.py:320
  149.0 0.1 bitcast_reduce_fusion
  149.1 0.7 copy.26
  (20 shorter events, 0.4 us)
Async XLA Ops:
  39.0 5.1 %copy-start = (bf16[4,128]{1,0:T(4,128)(2,1)S(1)}, bf16[4,128]{1,0:T(4,128)(2,1)}, u32[]{:S(2)}) copy-start(bf16[4,128]{1,0:T(4,128)(2,1)} %param.22) | copy-start | bytes 3076
  39.0 5.1 %copy-start.1 = (bf16[4,128]{1,0:T(4,128)(2,1)S(1)}, bf16[4,128]{1,0:T(4,128)(2,1)}, u32[]{:S(2)}) copy-start(bf16[4,128]{1,0:T(4,128)(2,1)} %param.21) | copy-start | bytes 3076
  39.0 5.1 %copy-start.2 = (bf16[4,128]{1,0:T(4,128)(2,1)S(1)}, bf16[4,128]{1,0:T(4,128)(2,1)}, u32[]{:S(2)}) copy-start(bf16[4,128]{1,0:T(4,128)(2,1)} %param.20) | copy-start | bytes 3076
  39.0 17.5 %all-to-all-start = ((bf16[4,1632,128]{2,1,0:T(8,128)(2,1)}), bf16[4,1632,128]{2,1,0:T(8,128)(2,1)S(1)}, u32[]{:S(2)}, u32[]{:S(2)}) async-start(bf16[4,1632,128]{2,1,0:T(8,128)(2,1)} %pad_maximum_fusion), calls=%async_computation | async-start | bytes 3342336 | tf_op jit(solution)/shard_map/all_to_all | solution.py:258
  82.6 5.3 %collective-permute-start = (bf16[8,1024]{1,0:T(8,128)(2,1)S(1)}, bf16[8,1024]{1,0:T(8,128)(2,1)S(1)}, u32[]{:S(2)}, u32[]{:S(2)}) collective-permute-start(bf16[8,1024]{1,0:T(8,128)(2,1)S(1)} %slice.9), channel_id=1, source_target_pairs={{0,32},{32,64},{64,96},{96,128},{128,160},{160,192},{192,224},{224... | collective-permute-start | bytes 49160 | tf_op jit(solution)/shard_map/ppermute | solution.py:262
  85.6 36.7 %copy-start.3 = (f32[128]{0:T(128)S(1)}, f32[128]{0:T(128)}, u32[]{:S(2)}) copy-start(f32[128]{0:T(128)} %param.24) | copy-start | bytes 1540
